TPU v7x, 32 devices: a whole 2x2x4 slice. The times are simulated.
32 devices in a mesh: grp: 2 (over y), sp: 4 (over z), tp: 4 (over x, core).
Axes of the slice: x: 2, y: 2, z: 4, core: 2. Of those that a mesh axis runs over, the one named last changes fastest.
Arguments:
- queries: bfloat16 [1024, 512], P(('grp', 'sp'), 'tp'), parts along dimension 0, may hold values from -6 to 6
- key_rows: bfloat16 [1024, 512], P(('grp', 'sp'), 'tp'), parts along dimension 0, may hold values from -6 to 6
- value_rows: bfloat16 [1024, 512], P(('grp', 'sp'), 'tp'), parts along dimension 0, may hold values from -16 to 16
- key_bias: bfloat16 [8, 1024], P('tp', ('grp', 'sp')), parts along dimension 1, may hold values from -20 to 0
- residual: bfloat16 [1024, 2048], P(('grp', 'sp')), parts along dimension 0, may hold values from -6 to 6
- out_weight: bfloat16 [512, 2048], P('tp'), may hold values from -0.25 to 0.25
- norm_gain: bfloat16 [2048], replicated, may hold values from 0.099609375 to 1.8984375
- gate_weight: bfloat16 [2048, 3072], P('sp', 'tp'), may hold values from -0.125 to 0.125
- up_weight: bfloat16 [2048, 3072], P('sp', 'tp'), may hold values from -0.125 to 0.125
- down_weight: bfloat16 [3072, 2048], P('tp', 'sp'), may hold values from -0.109375 to 0.109375
Outputs:
- layer_out: bfloat16 [1024, 2048], P(('grp', 'sp')), parts along dimension 0
There are 2 independent parts, one for each index of `grp`. A program takes and returns all parts, laid end to end along the dimension named above; an argument that names none is the same for every part. Nothing has to cross between parts.
All inputs are finite; a program needn't handle non-finite values.
Results may differ from a plain program's by a relative error of at most 0.014.
Values may be sent and summed in bfloat16 or wider, within the bound.
A program may use at most 64 MiB of HBM per device.

v0:
```python
import jax
import jax.numpy as jnp
from jax import lax
from jax.sharding import PartitionSpec as P

norm_eps = 1e-05


def from_behind(value, axis, steps):
    count = lax.axis_size(axis)
    initial, last = (max(0, -steps), min(count, count - steps))
    return lax.ppermute(value, axis, [(source, source + steps) for source in range(initial, last)])


def stick_block(carry, query_heads, key_block, value_block, bias_block, query_pos, key_start):
    accum, kept_log = carry
    key_count = key_block.shape[0]
    head_count = query_heads.shape[1]
    key_heads = key_block.reshape(key_count, head_count, -1)
    value_heads = value_block.reshape(key_count, head_count, -1)
    scale = key_heads.shape[2] ** (-0.5)
    scores = (
        jnp.einsum("qhd,khd->hqk", query_heads, key_heads, preferred_element_type=jnp.float32)
        * scale
    )
    scores = scores + bias_block.astype(jnp.float32)[:, None, :]
    key_pos = key_start + lax.iota(jnp.int32, key_count)
    strict = ((key_pos[None, :] < query_pos[:, None]) & (key_pos[None, :] >= 0))[None]
    log_retained = jnp.where(strict, jax.nn.log_sigmoid(-scores), 0.0)
    between = lax.cumsum(log_retained, axis=2, reverse=True) - log_retained + kept_log[:, :, None]
    stick = jnp.where(strict, jnp.exp(jax.nn.log_sigmoid(scores) + between), 0.0).astype(
        jnp.bfloat16
    )
    accum = accum + jnp.einsum(
        "hqk,khd->qhd", stick, value_heads, preferred_element_type=jnp.float32
    )
    return (accum, kept_log + jnp.sum(log_retained, axis=2))


def normalize(middle_wide, norm_gain):
    mean_square = jnp.mean(middle_wide * middle_wide, axis=1, keepdims=True)
    return (middle_wide * lax.rsqrt(mean_square + norm_eps) * norm_gain.astype(jnp.float32)).astype(
        jnp.bfloat16
    )


def body(
    queries,
    key_rows,
    value_rows,
    key_bias,
    residual,
    out_weight,
    norm_gain,
    gate_weight,
    up_weight,
    down_weight,
):
    seg_rows = queries.shape[0]
    head_count = key_bias.shape[0]
    head_width = queries.shape[1] // head_count
    sp_count = lax.axis_size("sp")
    token_place = lax.axis_index("sp")
    query_heads = queries.reshape(seg_rows, head_count, head_width)
    query_pos = token_place * seg_rows + lax.iota(jnp.int32, seg_rows)
    start_carry = (
        jnp.zeros((seg_rows, head_count, head_width), jnp.float32),
        jnp.zeros((head_count, seg_rows), jnp.float32),
    )
    carry = stick_block(
        start_carry, query_heads, key_rows, value_rows, key_bias, query_pos, token_place * seg_rows
    )

    def advance(hop_index, state):
        carry_now, blocks = state
        blocks = from_behind((blocks[0], blocks[1], blocks[2]), "sp", 1)

        def attend(current):
            return stick_block(
                current,
                query_heads,
                blocks[0],
                blocks[1],
                blocks[2],
                query_pos,
                (token_place - hop_index) * seg_rows,
            )

        carry_now = lax.cond(token_place >= hop_index, attend, lambda current: current, carry_now)
        return (carry_now, blocks)

    carry, passed_blocks = lax.fori_loop(
        1, sp_count, advance, (carry, (key_rows, value_rows, key_bias))
    )
    attended = carry[0].reshape(seg_rows, head_count * head_width).astype(jnp.bfloat16)
    own_rows = seg_rows // lax.axis_size("tp")
    own_start = lax.axis_index("tp") * own_rows
    mixed = lax.psum_scatter(
        jnp.dot(attended, out_weight, preferred_element_type=jnp.float32).astype(jnp.bfloat16),
        "tp",
        scatter_dimension=0,
        tiled=True,
    ).astype(jnp.float32)
    own_residual = lax.dynamic_slice_in_dim(residual, own_start, own_rows, 0)
    middle = (own_residual.astype(jnp.float32) + mixed).astype(jnp.bfloat16)
    middle_wide = middle.astype(jnp.float32)
    normed_all = lax.all_gather(normalize(middle_wide, norm_gain), "tp", axis=0, tiled=True)
    gate_pre = jnp.dot(
        normed_all,
        lax.all_gather(gate_weight, "sp", axis=0, tiled=True),
        preferred_element_type=jnp.float32,
    )
    up_pre = jnp.dot(
        normed_all,
        lax.all_gather(up_weight, "sp", axis=0, tiled=True),
        preferred_element_type=jnp.float32,
    )
    hidden = (jax.nn.silu(gate_pre) * up_pre).astype(jnp.bfloat16)
    down_terms = jnp.dot(
        hidden,
        lax.all_gather(down_weight, "sp", axis=1, tiled=True),
        preferred_element_type=jnp.float32,
    )
    down_sum = lax.psum_scatter(
        down_terms.astype(jnp.bfloat16), "tp", scatter_dimension=0, tiled=True
    ).astype(jnp.float32)
    own_out = (middle_wide + down_sum).astype(jnp.bfloat16)
    return lax.all_gather(own_out, "tp", axis=0, tiled=True)


def solution(mesh):
    in_specs = (
        P(("grp", "sp"), "tp"),
        P(("grp", "sp"), "tp"),
        P(("grp", "sp"), "tp"),
        P("tp", ("grp", "sp")),
        P(("grp", "sp"), None),
        P("tp", None),
        P(),
        P("sp", "tp"),
        P("sp", "tp"),
        P("tp", "sp"),
    )
    out_specs = P(("grp", "sp"), None)
    return jax.shard_map(body, mesh=mesh, in_specs=in_specs, out_specs=out_specs, check_vma=False)
```

profile of v0, /device:TPU:0, one launch (start us, length us, event | category | flops | bytes accessed | tf_op | source)
XLA Modules:
  0.0 288.5 jit_solution(2027559084728312409)
XLA Ops:
  7.4 0.7 copy.51
  8.1 0.9 copy.19
  9.0 0.9 copy.20
  9.9 0.9 copy.21
  10.7 0.1 compare_and_fusion.1
  10.8 0.2 fusion.33
  11.1 0.1 fusion.36
  11.2 2.2 reduce_window_sum.16
  13.4 0.3 convolution_bitcast_fusion.1
  13.7 38.2 %while.22 = (s32[]{:T(128)}, f32[128,2,64]{0,2,1:T(8,128)S(1)}, f32[2,128]{1,0:T(2,128)S(1)}, bf16[128,128]{0,1:T(8,128)(2,1)S(1)}, bf16[128,128]{0,1:T(8,128)(2...) while((s32[]{:T(128)}, f32[128,2,64]{0,2,1:T(8,128)S(1)}, ...), condition=%wide.region_7.8_spmd.clone, body=%wide.region_2.7_spmd.clone.sunk | while | flops 13992710 | bytes 1652875 | solution.py:92
  13.7 5.0 %collective-permute-start = (bf16[128,128]{0,1:T(8,128)(2,1)S(1)}, bf16[128,128]{0,1:T(8,128)(2,1)S(1)}, u32[]{:S(2)}, u32[]{:S(2)}) collective-permute-start(bf16[128,128]{0,1:T(8,128)(2,1)S(1)} %get-tuple-element.347), channel_id=1, source_target_pairs={{0,4},{4,8},{8,12},{1,5},{5,9},{9,13},{2,6},{6,10},{10,14},{3,7},{... | collective-permute-start | bytes 98312 | tf_op jit(solution)/shard_map/while/body/eval_jaxpr/ppermute | solution.py:12
  18.7 3.5 %collective-permute-start.2 = (bf16[128,128]{0,1:T(8,128)(2,1)S(1)}, bf16[128,128]{0,1:T(8,128)(2,1)S(1)}, u32[]{:S(2)}, u32[]{:S(2)}) collective-permute-start(bf16[128,128]{0,1:T(8,128)(2,1)S(1)} %get-tuple-element.348), channel_id=1, source_target_pairs={{0,4},{4,8},{8,12},{1,5},{5,9},{9,13},{2,6},{6,10},{10,14},{3,7},{... | collective-permute-start | bytes 98312 | tf_op jit(solution)/shard_map/while/body/eval_jaxpr/ppermute | solution.py:12
  22.2 3.5 %collective-permute-start.1 = (bf16[2,128]{1,0:T(2,128)(2,1)S(1)}, bf16[2,128]{1,0:T(2,128)(2,1)S(1)}, u32[]{:S(2)}, u32[]{:S(2)}) collective-permute-start(bf16[2,128]{1,0:T(2,128)(2,1)S(1)} %get-tuple-element.349), channel_id=1, source_target_pairs={{0,4},{4,8},{8,12},{1,5},{5,9},{9,13},{2,6},{6,10},{10,14},{3,7},{... | collective-permute-start | bytes 1544 | tf_op jit(solution)/shard_map/while/body/eval_jaxpr/ppermute | solution.py:12
  25.7 1.3 collective-permute-done.1
  27.0 0.0 collective-permute-done
  27.0 0.0 collective-permute-done.2
  27.0 7.2 %collective-permute-start = (bf16[128,128]{0,1:T(8,128)(2,1)S(1)}, bf16[128,128]{0,1:T(8,128)(2,1)S(1)}, u32[]{:S(2)}, u32[]{:S(2)}) collective-permute-start(bf16[128,128]{0,1:T(8,128)(2,1)S(1)} %get-tuple-element.347), channel_id=1, source_target_pairs={{0,4},{4,8},{8,12},{1,5},{5,9},{9,13},{2,6},{6,10},{10,14},{3,7},{... | collective-permute-start | bytes 98312 | tf_op jit(solution)/shard_map/while/body/eval_jaxpr/ppermute | solution.py:12
  34.3 1.9 collective-permute-start.2
  36.2 1.9 collective-permute-start.1
  38.2 1.3 collective-permute-done.1
  39.5 4.2 %collective-permute-start = (bf16[128,128]{0,1:T(8,128)(2,1)S(1)}, bf16[128,128]{0,1:T(8,128)(2,1)S(1)}, u32[]{:S(2)}, u32[]{:S(2)}) collective-permute-start(bf16[128,128]{0,1:T(8,128)(2,1)S(1)} %get-tuple-element.347), channel_id=1, source_target_pairs={{0,4},{4,8},{8,12},{1,5},{5,9},{9,13},{2,6},{6,10},{10,14},{3,7},{... | collective-permute-start | bytes 98312 | tf_op jit(solution)/shard_map/while/body/eval_jaxpr/ppermute | solution.py:12
  43.7 5.0 %collective-permute-start.2 = (bf16[128,128]{0,1:T(8,128)(2,1)S(1)}, bf16[128,128]{0,1:T(8,128)(2,1)S(1)}, u32[]{:S(2)}, u32[]{:S(2)}) collective-permute-start(bf16[128,128]{0,1:T(8,128)(2,1)S(1)} %get-tuple-element.348), channel_id=1, source_target_pairs={{0,4},{4,8},{8,12},{1,5},{5,9},{9,13},{2,6},{6,10},{10,14},{3,7},{... | collective-permute-start | bytes 98312 | tf_op jit(solution)/shard_map/while/body/eval_jaxpr/ppermute | solution.py:12
  48.7 1.9 collective-permute-start.1
  50.6 1.3 collective-permute-done.1
  52.0 0.0 copy-start.1
  52.0 1.1 convolution_convert_fusion.1
  53.1 0.0 reduce-scatter.3.cloned.1.call-update
  53.2 0.0 all-gather.4.cloned.1.call-start
  53.2 0.5 all-gather.4.cloned.1.call-update
  53.7 0.0 all-gather.6.cloned.1.call-start
  53.8 0.5 all-gather.6.cloned.1.call-update
  54.3 0.0 all-gather.8.cloned.1.call-start
  54.4 0.5 all-gather.8.cloned.1.call-update
  54.9 0.0 reduce-scatter.5.cloned.1.call-start
  55.0 21.9 %reduce-scatter.3.cloned.1.call-done = bf16[32,2048]{1,0:T(8,128)(2,1)} async-done(((bf16[128,2048]{1,0:T(8,128)(2,1)}), bf16[32,2048]{1,0:T(8,128)(2,1)}) %reduce-scatter.3.cloned.1.call-update) | async-done | bytes 131088 | tf_op jit(solution)/shard_map/reduce_scatter | solution.py:98
  76.9 1.1 fusion.21
  78.0 0.1 fusion.23
  78.1 6.6 %all_gather.15 = bf16[128,2048]{1,0:T(8,128)(2,1)S(1)} all-gather(bf16[32,2048]{1,0:T(8,128)(2,1)S(1)} %fusion.23), channel_id=1, replica_groups=mesh['grp'=2,'sp'=4,'tp'=4] {'tp'}, dimensions={0}, use_global_device_ids=true | all-gather | bytes 655360 | tf_op jit(solution)/shard_map/all_gather | solution.py:107
  84.7 35.7 %all-gather.4.cloned.1.call-done = bf16[2048,768]{1,0:T(8,128)(2,1)} async-done(((bf16[512,768]{1,0:T(8,128)(2,1)}), bf16[2048,768]{1,0:T(8,128)(2,1)}) %all-gather.4.cloned.1.call-update) | async-done | bytes 3145744 | tf_op jit(solution)/shard_map/all_gather | solution.py:110
  120.4 2.5 fusion.37
  122.9 60.9 %all-gather.6.cloned.1.call-done = bf16[2048,768]{1,0:T(8,128)(2,1)} async-done(((bf16[512,768]{1,0:T(8,128)(2,1)}), bf16[2048,768]{1,0:T(8,128)(2,1)}) %all-gather.6.cloned.1.call-update) | async-done | bytes 3145744 | tf_op jit(solution)/shard_map/all_gather | solution.py:115
  183.8 63.4 %all-gather.8.cloned.1.call-done = bf16[768,2048]{1,0:T(8,128)(2,1)} async-done(((bf16[768,512]{1,0:T(8,128)(2,1)}), bf16[768,2048]{1,0:T(8,128)(2,1)}) %all-gather.8.cloned.1.call-update) | async-done | bytes 3145744 | tf_op jit(solution)/shard_map/all_gather | solution.py:121
  247.3 4.9 %convolution_convert_fusion = bf16[128,2048]{1,0:T(8,128)(2,1)} fusion(bf16[768,2048]{1,0:T(8,128)(2,1)} %all-gather.8.cloned.1.call-done, bf16[128,2048]{1,0:T(8,128)(2,1)S(1)} %all_gather.15, bf16[2048,768]{1,0:T(8,128)(2,1)} %all-gather.6.cloned.1.call-done, f32[128,768]{1,0:T(8,128)S(1)} %fusion.37), kind=kOutput, calls=%fused_computation.22 | convolution fusion | flops 806158336 | bytes 7733248 | tf_op jit(solution)/shard_map/dot_general | solution.py:119
  252.2 0.0 reduce-scatter.5.cloned.1.call-update
  252.2 20.4 %reduce-scatter.5.cloned.1.call-done = bf16[32,2048]{1,0:T(8,128)(2,1)} async-done(((bf16[128,2048]{1,0:T(8,128)(2,1)}), bf16[32,2048]{1,0:T(8,128)(2,1)}) %reduce-scatter.5.cloned.1.call-update) | async-done | bytes 131088 | tf_op jit(solution)/shard_map/reduce_scatter | solution.py:124
  272.6 0.9 fusion.24
  273.6 6.6 %all_gather.19 = bf16[128,2048]{1,0:T(8,128)(2,1)S(1)} all-gather(bf16[32,2048]{1,0:T(8,128)(2,1)S(1)} %fusion.24), channel_id=1, replica_groups=mesh['grp'=2,'sp'=4,'tp'=4] {'tp'}, dimensions={0}, use_global_device_ids=true | all-gather | bytes 655360 | tf_op jit(solution)/shard_map/all_gather | solution.py:128
  280.2 0.8 copy.52
  (29 shorter events, 0.1 us)
Async XLA Ops:
  7.4 44.6 %copy-start = (bf16[128,2048]{1,0:T(8,128)(2,1)S(1)}, bf16[128,2048]{1,0:T(8,128)(2,1)}, u32[]{:S(2)}) copy-start(bf16[128,2048]{1,0:T(8,128)(2,1)} %param.19) | copy-start | bytes 1572868
  7.4 69.5 %reduce-scatter.3.cloned.1.call-start = ((), (), s32[]{:S(2)}) async-start(), calls=%async_computation.2 | async-start | bytes 655360 | tf_op jit(solution)/shard_map/reduce_scatter | solution.py:98
  13.7 13.2 %collective-permute-start = (bf16[128,128]{0,1:T(8,128)(2,1)S(1)}, bf16[128,128]{0,1:T(8,128)(2,1)S(1)}, u32[]{:S(2)}, u32[]{:S(2)}) collective-permute-start(bf16[128,128]{0,1:T(8,128)(2,1)S(1)} %get-tuple-element.347), channel_id=1, source_target_pairs={{0,4},{4,8},{8,12},{1,5},{5,9},{9,13},{2,6},{6,10},{10,14},{3,7},{... | collective-permute-start | bytes 98312 | tf_op jit(solution)/shard_map/while/body/eval_jaxpr/ppermute | solution.py:12
  18.7 8.3 %collective-permute-start.2 = (bf16[128,128]{0,1:T(8,128)(2,1)S(1)}, bf16[128,128]{0,1:T(8,128)(2,1)S(1)}, u32[]{:S(2)}, u32[]{:S(2)}) collective-permute-start(bf16[128,128]{0,1:T(8,128)(2,1)S(1)} %get-tuple-element.348), channel_id=1, source_target_pairs={{0,4},{4,8},{8,12},{1,5},{5,9},{9,13},{2,6},{6,10},{10,14},{3,7},{... | collective-permute-start | bytes 98312 | tf_op jit(solution)/shard_map/while/body/eval_jaxpr/ppermute | solution.py:12
  22.2 4.8 %collective-permute-start.1 = (bf16[2,128]{1,0:T(2,128)(2,1)S(1)}, bf16[2,128]{1,0:T(2,128)(2,1)S(1)}, u32[]{:S(2)}, u32[]{:S(2)}) collective-permute-start(bf16[2,128]{1,0:T(2,128)(2,1)S(1)} %get-tuple-element.349), channel_id=1, source_target_pairs={{0,4},{4,8},{8,12},{1,5},{5,9},{9,13},{2,6},{6,10},{10,14},{3,7},{... | collective-permute-start | bytes 1544 | tf_op jit(solution)/shard_map/while/body/eval_jaxpr/ppermute | solution.py:12
  27.0 12.4 %collective-permute-start = (bf16[128,128]{0,1:T(8,128)(2,1)S(1)}, bf16[128,128]{0,1:T(8,128)(2,1)S(1)}, u32[]{:S(2)}, u32[]{:S(2)}) collective-permute-start(bf16[128,128]{0,1:T(8,128)(2,1)S(1)} %get-tuple-element.347), channel_id=1, source_target_pairs={{0,4},{4,8},{8,12},{1,5},{5,9},{9,13},{2,6},{6,10},{10,14},{3,7},{... | collective-permute-start | bytes 98312 | tf_op jit(solution)/shard_map/while/body/eval_jaxpr/ppermute | solution.py:12
  34.3 5.1 %collective-permute-start.2 = (bf16[128,128]{0,1:T(8,128)(2,1)S(1)}, bf16[128,128]{0,1:T(8,128)(2,1)S(1)}, u32[]{:S(2)}, u32[]{:S(2)}) collective-permute-start(bf16[128,128]{0,1:T(8,128)(2,1)S(1)} %get-tuple-element.348), channel_id=1, source_target_pairs={{0,4},{4,8},{8,12},{1,5},{5,9},{9,13},{2,6},{6,10},{10,14},{3,7},{... | collective-permute-start | bytes 98312 | tf_op jit(solution)/shard_map/while/body/eval_jaxpr/ppermute | solution.py:12
  36.2 3.2 %collective-permute-start.1 = (bf16[2,128]{1,0:T(2,128)(2,1)S(1)}, bf16[2,128]{1,0:T(2,128)(2,1)S(1)}, u32[]{:S(2)}, u32[]{:S(2)}) collective-permute-start(bf16[2,128]{1,0:T(2,128)(2,1)S(1)} %get-tuple-element.349), channel_id=1, source_target_pairs={{0,4},{4,8},{8,12},{1,5},{5,9},{9,13},{2,6},{6,10},{10,14},{3,7},{... | collective-permute-start | bytes 1544 | tf_op jit(solution)/shard_map/while/body/eval_jaxpr/ppermute | solution.py:12
  39.5 12.4 %collective-permute-start = (bf16[128,128]{0,1:T(8,128)(2,1)S(1)}, bf16[128,128]{0,1:T(8,128)(2,1)S(1)}, u32[]{:S(2)}, u32[]{:S(2)}) collective-permute-start(bf16[128,128]{0,1:T(8,128)(2,1)S(1)} %get-tuple-element.347), channel_id=1, source_target_pairs={{0,4},{4,8},{8,12},{1,5},{5,9},{9,13},{2,6},{6,10},{10,14},{3,7},{... | collective-permute-start | bytes 98312 | tf_op jit(solution)/shard_map/while/body/eval_jaxpr/ppermute | solution.py:12
  43.7 8.2 %collective-permute-start.2 = (bf16[128,128]{0,1:T(8,128)(2,1)S(1)}, bf16[128,128]{0,1:T(8,128)(2,1)S(1)}, u32[]{:S(2)}, u32[]{:S(2)}) collective-permute-start(bf16[128,128]{0,1:T(8,128)(2,1)S(1)} %get-tuple-element.348), channel_id=1, source_target_pairs={{0,4},{4,8},{8,12},{1,5},{5,9},{9,13},{2,6},{6,10},{10,14},{3,7},{... | collective-permute-start | bytes 98312 | tf_op jit(solution)/shard_map/while/body/eval_jaxpr/ppermute | solution.py:12
  48.7 3.2 %collective-permute-start.1 = (bf16[2,128]{1,0:T(2,128)(2,1)S(1)}, bf16[2,128]{1,0:T(2,128)(2,1)S(1)}, u32[]{:S(2)}, u32[]{:S(2)}) collective-permute-start(bf16[2,128]{1,0:T(2,128)(2,1)S(1)} %get-tuple-element.349), channel_id=1, source_target_pairs={{0,4},{4,8},{8,12},{1,5},{5,9},{9,13},{2,6},{6,10},{10,14},{3,7},{... | collective-permute-start | bytes 1544 | tf_op jit(solution)/shard_map/while/body/eval_jaxpr/ppermute | solution.py:12
  52.0 3.0 %copy-start.1 = (bf16[2048]{0:T(1024)(128)(2,1)S(1)}, bf16[2048]{0:T(1024)(128)(2,1)}, u32[]{:S(2)}) copy-start(bf16[2048]{0:T(1024)(128)(2,1)} %param.20) | copy-start | bytes 12292
  53.2 67.3 %all-gather.4.cloned.1.call-start = ((), (), s32[]{:S(2)}) async-start(), calls=%async_computation.3 | async-start | bytes 3932160 | tf_op jit(solution)/shard_map/all_gather | solution.py:110
  53.7 130.1 %all-gather.6.cloned.1.call-start = ((), (), s32[]{:S(2)}) async-start(), calls=%async_computation.4 | async-start | bytes 3932160 | tf_op jit(solution)/shard_map/all_gather | solution.py:115
  54.3 192.9 %all-gather.8.cloned.1.call-start = ((), (), s32[]{:S(2)}) async-start(), calls=%async_computation.5 | async-start | bytes 3932160 | tf_op jit(solution)/shard_map/all_gather | solution.py:121
  54.9 217.7 %reduce-scatter.5.cloned.1.call-start = ((), (), s32[]{:S(2)}) async-start(), calls=%async_computation.6 | async-start | bytes 655360 | tf_op jit(solution)/shard_map/reduce_scatter | solution.py:124
Sparse Core Ops, SparseCore 0:
  53.3 23.5 reduce-scatter.2
  252.3 20.2 reduce-scatter.4
Sparse Core Ops, SparseCore 1:
  55.2 65.2 all-gather.3
  121.9 61.9 all-gather.5
  185.3 61.9 all-gather.7
where the time goes:
time: 289 us
  waiting for transfers between devices  208 us (72%)
  starting transfers between devices  34.3 us (12%)
  between operations  15.1 us (5%)
  blocking collectives  13.2 us (5%)
  matrix products  9.04 us (3%)
  other arithmetic  4.64 us (2%)
  local copies, waits for them, and re-layouts  4.15 us (1%)
    all_gather x1, waiting for transfers between devices, body(): lax.all_gather(down_weight, 'sp', axis=1, tiled=True)  63.4 us
    all_gather x1, waiting for transfers between devices, body(): lax.all_gather(up_weight, 'sp', axis=0, tiled=True)  60.9 us
    all_gather x1, waiting for transfers between devices, body(): lax.all_gather(gate_weight, 'sp', axis=0, tiled=True)  35.7 us
    ppermute x9, starting transfers between devices, from_behind(): lax.ppermute(value, axis, [(source, source + steps) for source in range(i...  34.1 us
    reduce_scatter x1, waiting for transfers between devices, body(): lax.psum_scatter(jnp.dot(attended, out_weight, preferred_element_type=jnp...  21.9 us
    reduce_scatter x1, waiting for transfers between devices, body(): lax.psum_scatter(down_terms.astype(jnp.bfloat16), 'tp', scatter_dimension...  20.4 us
    all_gather x1, blocking collectives, body(): lax.all_gather(normalize(middle_wide, norm_gain), 'tp', axis=0, tiled=True)  6.6 us
    all_gather x1, blocking collectives, body(): return lax.all_gather(own_out, 'tp', axis=0, tiled=True)  6.58 us
  transfers between devices with their start and end apart: 14, of which 8 were waited for; matrix products, arithmetic and copies ran while one was open for 1% of the time, Pallas kernels for 0%

commit v1 on v0

--- a/solution.py
+++ b/solution.py
@@ -1,6 +1,10 @@
+import functools
+
 import jax
 import jax.numpy as jnp
 from jax import lax
+from jax.experimental import pallas as pl
+from jax.experimental.pallas import tpu as pltpu
 from jax.sharding import PartitionSpec as P
 
 norm_eps = 1e-05
@@ -128,6 +132,388 @@
     return lax.all_gather(own_out, "tp", axis=0, tiled=True)
 
 
+def contract(left, right, dims):
+    return lax.dot_general(left, right, ((dims[:1], dims[1:]), ((), ())), preferred_element_type=jnp.float32)
+
+
+def layer_kernel(
+    grp_count,
+    sp_count,
+    tp_count,
+    q_ref,
+    k_ref,
+    v_ref,
+    bias_ref,
+    res_ref,
+    ow_ref,
+    gain_ref,
+    gate_ref,
+    up_ref,
+    down_ref,
+    out_ref,
+    kbuf,
+    vbuf,
+    bbuf,
+    acc,
+    kept,
+    wsend,
+    w_all,
+    pbuf,
+    rbuf,
+    middle,
+    n_all,
+    h_all,
+    dbuf,
+    rdown,
+    zsend,
+    zin,
+    kv_sems,
+    w_sems,
+    wy_sems,
+    r_sems,
+    n_sems,
+    f_sems,
+    h_sems,
+    d_sems,
+    z_sems,
+    o_sems,
+):
+    g, s, t = lax.axis_index("grp"), lax.axis_index("sp"), lax.axis_index("tp")
+    rows, model = res_ref.shape
+    quarter = rows // tp_count
+    slab = model // sp_count
+    piece = gate_ref.shape[1] // sp_count
+    head_count = bias_ref.shape[0]
+    width = q_ref.shape[1] // head_count
+    sends = []
+
+    def sp_peer(step):
+        return lax.rem(s + step + sp_count, sp_count)
+
+    def tp_peer(step):
+        return lax.rem(t + step + tp_count, tp_count)
+
+    core_mate = t + 1 - 2 * lax.rem(t, 2)
+    far_mate = lax.rem(t + 2, 4)
+
+    def copy(source, target, sems, index, device):
+        return pltpu.make_async_remote_copy(
+            src_ref=source,
+            dst_ref=target,
+            send_sem=sems.at[(0,) + index],
+            recv_sem=sems.at[(1,) + index],
+            device_id=device,
+            device_id_type=pl.DeviceIdType.MESH,
+        )
+
+    def launch(*arguments):
+        made = copy(*arguments)
+        made.start()
+        sends.append(made)
+        return made
+
+    barrier = pltpu.get_barrier_semaphore()
+    for step in range(1, sp_count):
+        pl.semaphore_signal(barrier, inc=1, device_id=(g, sp_peer(step), t), device_id_type=pl.DeviceIdType.MESH)
+    for step in range(1, tp_count):
+        pl.semaphore_signal(barrier, inc=1, device_id=(g, s, tp_peer(step)), device_id_type=pl.DeviceIdType.MESH)
+    pl.semaphore_signal(barrier, inc=1, device_id=(1 - g, s, t), device_id_type=pl.DeviceIdType.MESH)
+    pl.semaphore_wait(barrier, sp_count + tp_count - 1)
+
+    kv_copies = {}
+    for step in range(1, sp_count):
+        device = (g, sp_peer(step), t)
+        kv_copies[step] = [
+            copy(k_ref, kbuf.at[step - 1], kv_sems, (0, step - 1), device),
+            copy(v_ref, vbuf.at[step - 1], kv_sems, (1, step - 1), device),
+            copy(bias_ref, bbuf.at[step - 1], kv_sems, (2, step - 1), device),
+        ]
+
+        @pl.when(s + step < sp_count)
+        def _():
+            for made in kv_copies[step]:
+                made.start()
+
+    for part, ref in ((0, gate_ref), (1, up_ref)):
+        for start in range(0, ref.shape[1], 128):
+            wsend[part, start : start + 128, :] = ref[:, start : start + 128].T
+    w_copies = {}
+    for step in range(1, sp_count):
+        dest = sp_peer(step)
+        w_copies[step] = launch(
+            wsend.at[g, pl.ds(pl.multiple_of(dest * piece, 16), piece)],
+            w_all.at[s, g],
+            w_sems,
+            (step - 1,),
+            (g, dest, t),
+        )
+    for part in range(2):
+        w_all[s, part] = wsend[part, pl.ds(pl.multiple_of(s * piece, 16), piece), :]
+
+    acc[...] = jnp.zeros_like(acc)
+    kept[...] = jnp.zeros_like(kept)
+    query = q_ref[...]
+    lane = lax.broadcasted_iota(jnp.int32, query.shape, 1)
+    row_id = lax.broadcasted_iota(jnp.int32, (rows, rows), 0)
+    col_id = lax.broadcasted_iota(jnp.int32, (rows, rows), 1)
+    later = (row_id > col_id).astype(jnp.bfloat16)
+    scale = width ** (-0.5)
+
+    def attend(key_block, value_block, bias_block, diagonal):
+        bias_wide = bias_block.astype(jnp.float32)
+        for head in range(head_count):
+            mine = (lane >= head * width) & (lane < (head + 1) * width)
+            zero = jnp.zeros_like(query)
+            scores = contract(jnp.where(mine, query, zero), key_block, (1, 1)) * scale
+            scores = scores + bias_wide[head : head + 1, :]
+            soft = jnp.log1p(jnp.exp(-jnp.abs(scores)))
+            log_take = jnp.minimum(scores, 0.0) - soft
+            log_keep = -jnp.maximum(scores, 0.0) - soft
+            if diagonal:
+                log_keep = jnp.where(col_id < row_id, log_keep, 0.0)
+            high = log_keep.astype(jnp.bfloat16)
+            low = (log_keep - high.astype(jnp.float32)).astype(jnp.bfloat16)
+            between = contract(high, later, (1, 0)) + contract(low, later, (1, 0)) + kept[head]
+            stick = jnp.exp(log_take + between)
+            if diagonal:
+                stick = jnp.where(col_id < row_id, stick, 0.0)
+            acc[...] += contract(
+                stick.astype(jnp.bfloat16), jnp.where(mine, value_block, zero), (1, 0)
+            )
+            kept[head] = kept[head] + jnp.sum(log_keep, axis=1, keepdims=True)
+
+    attend(k_ref[...], v_ref[...], bias_ref[...], True)
+    for step in range(1, sp_count):
+
+        @pl.when(s >= step)
+        def _():
+            for made in kv_copies[step]:
+                made.wait_recv()
+            attend(kbuf[step - 1], vbuf[step - 1], bbuf[step - 1], False)
+
+    attended = acc[...].astype(jnp.bfloat16)
+    for start in range(0, model, 512):
+        pbuf[:, start : start + 512] = contract(
+            attended, ow_ref[:, start : start + 512], (1, 0)
+        ).astype(jnp.bfloat16)
+
+    def own_rows(index):
+        return pl.ds(pl.multiple_of(index * quarter, quarter), quarter)
+
+    r_copies = []
+    for step in range(1, tp_count):
+        dest = tp_peer(step)
+        r_copies.append(
+            launch(pbuf.at[own_rows(dest)], rbuf.at[step - 1], r_sems, (step - 1,), (g, s, dest))
+        )
+    mixed = pbuf[own_rows(t), :].astype(jnp.float32)
+    for index, made in enumerate(r_copies):
+        made.wait_recv()
+        mixed = mixed + rbuf[index].astype(jnp.float32)
+    middle[...] = (res_ref[own_rows(t), :].astype(jnp.float32) + mixed).astype(jnp.bfloat16)
+    wide = middle[...].astype(jnp.float32)
+    mean_square = jnp.mean(wide * wide, axis=1, keepdims=True)
+    n_all[s, t] = (
+        wide * lax.rsqrt(mean_square + norm_eps) * gain_ref[...].astype(jnp.float32)
+    ).astype(jnp.bfloat16)
+
+    n_copies = {}
+    for step in range(1, sp_count):
+        n_copies[step] = launch(
+            n_all.at[s, t], n_all.at[s, t], n_sems, (step - 1,), (g, sp_peer(step), t)
+        )
+
+    def spread(ref, sems, index):
+        return (
+            launch(ref(t), ref(t), sems, (0, index), (g, s, far_mate)),
+            launch(ref(t), ref(t), sems, (1, index), (g, s, core_mate)),
+        )
+
+    def finish(ref, sems, index, first):
+        first[0].wait_recv()
+        relayed = launch(ref(far_mate), ref(far_mate), sems, (2, index), (g, s, core_mate))
+        first[1].wait_recv()
+        relayed.wait_recv()
+
+    def n_view(block):
+        return lambda place: n_all.at[block, place]
+
+    spreads = {0: spread(n_view(s), f_sems, 0)}
+    y_copies = []
+    for step in range(1, sp_count):
+        w_copies[step].wait_recv()
+        view = w_all.at[sp_peer(-step), g]
+        y_copies.append(launch(view, view, wy_sems, (step - 1,), (1 - g, s, t)))
+    for step in range(1, sp_count):
+        n_copies[step].wait_recv()
+        spreads[step] = spread(n_view(sp_peer(-step)), f_sems, step)
+    for made in y_copies:
+        made.wait_recv()
+
+    h_copies = {}
+    for step in range(sp_count):
+        block = sp_peer(-step)
+        finish(n_view(block), f_sems, step, spreads[step])
+        total = jnp.zeros((2 * piece, rows), jnp.float32)
+        tokens = n_all[block].reshape(rows, model)
+        for part in range(sp_count):
+            total = total + contract(
+                w_all[part].reshape(2 * piece, slab),
+                tokens[:, part * slab : (part + 1) * slab],
+                (1, 1),
+            )
+        gate_pre, up_pre = total[:piece], total[piece:]
+        h_all[block, s] = (gate_pre / (1.0 + jnp.exp(-gate_pre)) * up_pre).astype(jnp.bfloat16)
+        for hop in range(1, sp_count):
+            h_copies[step, hop] = launch(
+                h_all.at[block, s], h_all.at[block, s], h_sems, (step, hop - 1), (g, sp_peer(hop), t)
+            )
+
+    d_copies = {}
+    order = list(range(1, sp_count)) + [0]
+    for step in order:
+        block = sp_peer(-step)
+        for hop in range(1, sp_count):
+            h_copies[(step - hop) % sp_count, hop].wait_recv()
+        hidden = h_all[block].reshape(sp_count * piece, rows)
+        dbuf[block] = contract(hidden, down_ref[...], (0, 0)).astype(jnp.bfloat16)
+        for hop in range(1, tp_count):
+            dest = tp_peer(hop)
+            d_copies[step, hop] = launch(
+                dbuf.at[block, own_rows(dest)],
+                rdown.at[hop - 1, step],
+                d_sems,
+                (step, hop - 1),
+                (g, s, dest),
+            )
+    z_copies = {}
+    for step in order:
+        block = sp_peer(-step)
+        summed = dbuf[block, own_rows(t), :].astype(jnp.float32)
+        for hop in range(1, tp_count):
+            d_copies[step, hop].wait_recv()
+            summed = summed + rdown[hop - 1, step].astype(jnp.float32)
+        if step:
+            zsend[step - 1] = summed.astype(jnp.bfloat16)
+            z_copies[step] = launch(
+                zsend.at[step - 1], zin.at[s], z_sems, (step - 1,), (g, block, t)
+            )
+        else:
+            zin[s] = summed.astype(jnp.bfloat16)
+    for step in range(1, sp_count):
+        z_copies[step].wait_recv()
+    for part in range(sp_count):
+        cols = slice(part * slab, (part + 1) * slab)
+        out_ref[own_rows(t), cols] = (
+            middle[:, cols].astype(jnp.float32) + zin[part].astype(jnp.float32)
+        ).astype(jnp.bfloat16)
+
+    def out_view(place):
+        return out_ref.at[own_rows(place)]
+
+    finish(out_view, o_sems, 0, spread(out_view, o_sems, 0))
+    for made in sends:
+        made.wait_send()
+    for step in range(1, sp_count):
+
+        @pl.when(s + step < sp_count)
+        def _():
+            for made in kv_copies[step]:
+                made.wait_send()
+
+
+def fused_body(
+    grp_count,
+    sp_count,
+    tp_count,
+    queries,
+    key_rows,
+    value_rows,
+    key_bias,
+    residual,
+    out_weight,
+    norm_gain,
+    gate_weight,
+    up_weight,
+    down_weight,
+):
+    rows, columns = queries.shape
+    head_count = key_bias.shape[0]
+    model = residual.shape[1]
+    hidden = gate_weight.shape[1]
+    piece, slab, quarter = hidden // sp_count, model // sp_count, rows // tp_count
+    n, m = sp_count - 1, tp_count - 1
+    half, wide = jnp.bfloat16, jnp.float32
+    dma = pltpu.SemaphoreType.DMA
+    return pl.pallas_call(
+        functools.partial(layer_kernel, grp_count, sp_count, tp_count),
+        out_shape=jax.ShapeDtypeStruct((rows, model), half),
+        in_specs=[pl.BlockSpec(memory_space=pltpu.VMEM)] * 10,
+        out_specs=pl.BlockSpec(memory_space=pltpu.VMEM),
+        scratch_shapes=[
+            pltpu.VMEM((n, rows, columns), half),
+            pltpu.VMEM((n, rows, columns), half),
+            pltpu.VMEM((n, head_count, rows), half),
+            pltpu.VMEM((rows, columns), wide),
+            pltpu.VMEM((head_count, rows, 1), wide),
+            pltpu.VMEM((2, hidden, slab), half),
+            pltpu.VMEM((sp_count, 2, piece, slab), half),
+            pltpu.VMEM((rows, model), half),
+            pltpu.VMEM((m, quarter, model), half),
+            pltpu.VMEM((quarter, model), half),
+            pltpu.VMEM((sp_count, tp_count, quarter, model), half),
+            pltpu.VMEM((sp_count, sp_count, piece, rows), half),
+            pltpu.VMEM((sp_count, rows, slab), half),
+            pltpu.VMEM((m, sp_count, quarter, slab), half),
+            pltpu.VMEM((n, quarter, slab), half),
+            pltpu.VMEM((sp_count, quarter, slab), half),
+            dma((2, 3, n)),
+            dma((2, n)),
+            dma((2, n)),
+            dma((2, m)),
+            dma((2, n)),
+            dma((2, 3, sp_count)),
+            dma((2, sp_count, n)),
+            dma((2, sp_count, m)),
+            dma((2, n)),
+            dma((2, 3, 1)),
+        ],
+        compiler_params=pltpu.CompilerParams(
+            collective_id=0, has_side_effects=True, vmem_limit_bytes=48 * 1024 * 1024
+        ),
+    )(
+        queries,
+        key_rows,
+        value_rows,
+        key_bias,
+        residual,
+        out_weight,
+        norm_gain.reshape(1, model),
+        gate_weight,
+        up_weight,
+        down_weight,
+    )
+
+
+def any_body(sizes, *arguments):
+    grp_count, sp_count, tp_count = sizes
+    queries, model, hidden = arguments[0], arguments[4].shape[1], arguments[7].shape[1]
+    rows = queries.shape[0]
+    fits = (
+        grp_count == 2
+        and tp_count == 4
+        and 1 < sp_count <= 4
+        and rows == 128
+        and queries.shape[1] == 128
+        and (model // sp_count) % 128 == 0
+        and (hidden // sp_count) % 16 == 0
+        and hidden % 128 == 0
+    )
+    if fits:
+        return fused_body(grp_count, sp_count, tp_count, *arguments)
+    return body(*arguments)
+
+
 def solution(mesh):
     in_specs = (
         P(("grp", "sp"), "tp"),
@@ -142,4 +528,5 @@
         P("tp", "sp"),
     )
     out_specs = P(("grp", "sp"), None)
-    return jax.shard_map(body, mesh=mesh, in_specs=in_specs, out_specs=out_specs, check_vma=False)
+    sizes = tuple(mesh.shape[name] for name in ("grp", "sp", "tp"))
+    return jax.shard_map(functools.partial(any_body, sizes), mesh=mesh, in_specs=in_specs, out_specs=out_specs, check_vma=False)

time: 289 us -> 89.3 us (0.31)
  waiting for transfers between devices: 208 us -> 0 us
  Pallas kernels: 0 us -> 78.4 us
  starting transfers between devices: 34.3 us -> 0 us
  between operations: 15.1 us -> 0.03 us
  blocking collectives: 13.2 us -> 0 us
  matrix products: 9.04 us -> 0 us
  local copies, waits for them, and re-layouts: 4.15 us -> 9.25 us
  other arithmetic: 4.64 us -> 0 us
    all_gather x3 -> x0, waiting for transfers between devices: 160 us -> none  [the longest x1 63.4 us: body(): lax.all_gather(down_weight, 'sp', axis=1, tiled=True)]
    pallas_call x0 -> x1, Pallas kernels: none -> 78.4 us  [fused_body(): pl.pallas_call(functools.partial(layer_kernel, grp_count, sp_count, tp_co...]
    reduce_scatter x2 -> x0, waiting for transfers between devices: 42.3 us -> none  [the longest x1 21.9 us: body(): lax.psum_scatter(jnp.dot(attended, out_weight, preferred_element_type=jnp...]
    ppermute x9 -> x0, starting transfers between devices: 34.1 us -> none  [from_behind(): lax.ppermute(value, axis, [(source, source + steps) for source in range(i...]
    all_gather x2 -> x0, blocking collectives: 13.2 us -> none  [the longest x1 6.6 us: body(): lax.all_gather(normalize(middle_wide, norm_gain), 'tp', axis=0, tiled=True)]
    dot_general x5 -> x0, matrix products: 9.04 us -> none  [the longest x1 4.91 us: body(): jnp.dot(hidden, lax.all_gather(down_weight, 'sp', axis=1, tiled=True), pr...]
    unnamed x9 -> x19, local copies, waits for them, and re-layouts: 4.11 us -> 8.55 us
    ppermute x9 -> x0, waiting for transfers between devices: 3.83 us -> none  [from_behind(): lax.ppermute(value, axis, [(source, source + steps) for source in range(i...]
  transfers between devices with their start and end apart: 14 -> 0, of which waited for: 8 -> 0; matrix products, arithmetic and copies ran while one was open for 1% -> 0% of each run, Pallas kernels for 0% -> 0%
where the time goes in v1:
time: 89.3 us; the launch traced here: 87.7 us
  Pallas kernels  78.4 us (88%)
  local copies, waits for them, and re-layouts  9.25 us (10%)
    pallas_call x1, Pallas kernels, fused_body(): pl.pallas_call(functools.partial(layer_kernel, grp_count, sp_count, tp_co...  78.4 us
    unnamed x19, local copies, waits for them, and re-layouts  8.55 us

profile of v1, /device:TPU:0, one launch (start us, length us, event | category | flops | bytes accessed | tf_op | source)
XLA Modules:
  0.0 87.7 jit_solution(12615002912738955085)
XLA Ops:
  0.0 0.0 copy-start.8
  0.0 0.7 reshape.3.gain_ref
  0.7 0.0 copy-done.8
  0.7 0.0 copy-start
  0.7 1.1 %copy-done = bf16[512,768]{1,0:T(8,128)(2,1)S(1)} copy-done((bf16[512,768]{1,0:T(8,128)(2,1)S(1)}, bf16[512,768]{1,0:T(8,128)(2,1)}, u32[]{:S(2)}) %copy-start) | copy-done | bytes 786456
  1.9 0.0 copy-start.1
  1.9 1.1 %copy-done.1 = bf16[512,768]{1,0:T(8,128)(2,1)S(1)} copy-done((bf16[512,768]{1,0:T(8,128)(2,1)S(1)}, bf16[512,768]{1,0:T(8,128)(2,1)}, u32[]{:S(2)}) %copy-start.1) | copy-done | bytes 786456
  3.0 0.0 copy-start.2
  3.0 1.1 %copy-done.2 = bf16[768,512]{1,0:T(8,128)(2,1)S(1)} copy-done((bf16[768,512]{1,0:T(8,128)(2,1)S(1)}, bf16[768,512]{1,0:T(8,128)(2,1)}, u32[]{:S(2)}) %copy-start.2) | copy-done | bytes 786456
  4.1 0.0 copy-start.3
  4.1 1.0 %copy-done.3 = bf16[128,2048]{1,0:T(8,128)(2,1)S(1)} copy-done((bf16[128,2048]{1,0:T(8,128)(2,1)S(1)}, bf16[128,2048]{1,0:T(8,128)(2,1)}, u32[]{:S(2)}) %copy-start.3) | copy-done | bytes 524312
  5.2 0.0 copy-start.4
  5.2 1.0 %copy-done.4 = bf16[128,2048]{1,0:T(8,128)(2,1)S(1)} copy-done((bf16[128,2048]{1,0:T(8,128)(2,1)S(1)}, bf16[128,2048]{1,0:T(8,128)(2,1)}, u32[]{:S(2)}) %copy-start.4) | copy-done | bytes 524312
  6.2 0.0 copy-start.5
  6.2 0.8 copy-done.5
  7.0 0.0 copy-start.6
  7.0 0.8 copy-done.6
  7.7 0.0 copy-start.7
  7.7 0.8 copy-done.7
  8.5 78.4 %shard_map.100 = bf16[128,2048]{1,0:T(8,128)(2,1)S(1)} custom-call(bf16[128,128]{1,0:T(8,128)(2,1)S(1)} %copy-done.5, bf16[128,128]{1,0:T(8,128)(2,1)S(1)} %copy-done.6, bf16[128,128]{1,0:T(8,128)(2,1)S(1)} %copy-done.7, bf16[2,128]{1,0:T(2,128)(2,1)S(1)} %copy-done.8, bf16[128,2048]{1,0:T(8,128)(2,1)S(1)} %copy-done.3, bf16[128,2048]{1,0:T(8,128)(2,1)S(1)} %copy-done.4, ...), custom_call_target="tpu_custom_call" | custom-call | tf_op jit(solution)/shard_map/pallas_call | solution.py:448
  86.9 0.8 copy.12
Async XLA Ops:
  0.0 0.7 copy-start.8
  0.7 1.1 %copy-start = (bf16[512,768]{1,0:T(8,128)(2,1)S(1)}, bf16[512,768]{1,0:T(8,128)(2,1)}, u32[]{:S(2)}) copy-start(bf16[512,768]{1,0:T(8,128)(2,1)} %gate_ref.1) | copy-start | bytes 2359300
  1.9 1.1 %copy-start.1 = (bf16[512,768]{1,0:T(8,128)(2,1)S(1)}, bf16[512,768]{1,0:T(8,128)(2,1)}, u32[]{:S(2)}) copy-start(bf16[512,768]{1,0:T(8,128)(2,1)} %up_ref.1) | copy-start | bytes 2359300
  3.0 1.1 %copy-start.2 = (bf16[768,512]{1,0:T(8,128)(2,1)S(1)}, bf16[768,512]{1,0:T(8,128)(2,1)}, u32[]{:S(2)}) copy-start(bf16[768,512]{1,0:T(8,128)(2,1)} %down_ref.1) | copy-start | bytes 2359300
  4.1 1.0 %copy-start.3 = (bf16[128,2048]{1,0:T(8,128)(2,1)S(1)}, bf16[128,2048]{1,0:T(8,128)(2,1)}, u32[]{:S(2)}) copy-start(bf16[128,2048]{1,0:T(8,128)(2,1)} %res_ref.1) | copy-start | bytes 1572868
  5.2 1.0 %copy-start.4 = (bf16[128,2048]{1,0:T(8,128)(2,1)S(1)}, bf16[128,2048]{1,0:T(8,128)(2,1)}, u32[]{:S(2)}) copy-start(bf16[128,2048]{1,0:T(8,128)(2,1)} %ow_ref.1) | copy-start | bytes 1572868
  6.2 0.8 copy-start.5
  7.0 0.8 copy-start.6
  7.7 0.8 copy-start.7

commit v2 on v1

--- a/solution.py
+++ b/solution.py
@@ -140,6 +140,17 @@
     grp_count,
     sp_count,
     tp_count,
+    q_in,
+    k_in,
+    v_in,
+    bias_in,
+    res_in,
+    ow_in,
+    gain_in,
+    gate_in,
+    up_in,
+    down_in,
+    out_ref,
     q_ref,
     k_ref,
     v_ref,
@@ -150,7 +161,7 @@
     gate_ref,
     up_ref,
     down_ref,
-    out_ref,
+    load_sems,
     kbuf,
     vbuf,
     bbuf,
@@ -179,7 +190,7 @@
     o_sems,
 ):
     g, s, t = lax.axis_index("grp"), lax.axis_index("sp"), lax.axis_index("tp")
-    rows, model = res_ref.shape
+    rows, model = res_in.shape
     quarter = rows // tp_count
     slab = model // sp_count
     piece = gate_ref.shape[1] // sp_count
@@ -212,6 +223,25 @@
         sends.append(made)
         return made
 
+    own_part = res_in.at[pl.ds(pl.multiple_of(t * quarter, quarter), quarter)]
+    loads = {}
+    for index, (name, source, target) in enumerate(
+        (
+            ("k", k_in, k_ref),
+            ("v", v_in, v_ref),
+            ("bias", bias_in, bias_ref),
+            ("gate", gate_in, gate_ref),
+            ("up", up_in, up_ref),
+            ("q", q_in, q_ref),
+            ("ow", ow_in, ow_ref),
+            ("res", own_part, res_ref),
+            ("gain", gain_in, gain_ref),
+            ("down", down_in, down_ref),
+        )
+    ):
+        loads[name] = pltpu.make_async_copy(source, target, load_sems.at[index])
+        loads[name].start()
+
     barrier = pltpu.get_barrier_semaphore()
     for step in range(1, sp_count):
         pl.semaphore_signal(barrier, inc=1, device_id=(g, sp_peer(step), t), device_id_type=pl.DeviceIdType.MESH)
@@ -220,6 +250,8 @@
     pl.semaphore_signal(barrier, inc=1, device_id=(1 - g, s, t), device_id_type=pl.DeviceIdType.MESH)
     pl.semaphore_wait(barrier, sp_count + tp_count - 1)
 
+    for name in ("k", "v", "bias"):
+        loads[name].wait()
     kv_copies = {}
     for step in range(1, sp_count):
         device = (g, sp_peer(step), t)
@@ -234,6 +266,8 @@
             for made in kv_copies[step]:
                 made.start()
 
+    for name in ("gate", "up", "q"):
+        loads[name].wait()
     for part, ref in ((0, gate_ref), (1, up_ref)):
         for start in range(0, ref.shape[1], 128):
             wsend[part, start : start + 128, :] = ref[:, start : start + 128].T
@@ -291,6 +325,8 @@
                 made.wait_recv()
             attend(kbuf[step - 1], vbuf[step - 1], bbuf[step - 1], False)
 
+    for name in ("ow", "res", "gain", "down"):
+        loads[name].wait()
     attended = acc[...].astype(jnp.bfloat16)
     for start in range(0, model, 512):
         pbuf[:, start : start + 512] = contract(
@@ -310,11 +346,11 @@
     for index, made in enumerate(r_copies):
         made.wait_recv()
         mixed = mixed + rbuf[index].astype(jnp.float32)
-    middle[...] = (res_ref[own_rows(t), :].astype(jnp.float32) + mixed).astype(jnp.bfloat16)
+    middle[...] = (res_ref[...].astype(jnp.float32) + mixed).astype(jnp.bfloat16)
     wide = middle[...].astype(jnp.float32)
     mean_square = jnp.mean(wide * wide, axis=1, keepdims=True)
     n_all[s, t] = (
-        wide * lax.rsqrt(mean_square + norm_eps) * gain_ref[...].astype(jnp.float32)
+        wide * lax.rsqrt(mean_square + norm_eps) * gain_ref[...].astype(jnp.float32).reshape(1, model)
     ).astype(jnp.bfloat16)
 
     n_copies = {}
@@ -344,15 +380,21 @@
         w_copies[step].wait_recv()
         view = w_all.at[sp_peer(-step), g]
         y_copies.append(launch(view, view, wy_sems, (step - 1,), (1 - g, s, t)))
-    for step in range(1, sp_count):
-        n_copies[step].wait_recv()
-        spreads[step] = spread(n_view(sp_peer(-step)), f_sems, step)
+
+    def pass_on(step):
+        if step < sp_count:
+            n_copies[step].wait_recv()
+            spreads[step] = spread(n_view(sp_peer(-step)), f_sems, step)
+
+    pass_on(1)
     for made in y_copies:
         made.wait_recv()
 
     h_copies = {}
     for step in range(sp_count):
         block = sp_peer(-step)
+        if step:
+            pass_on(step + 1)
         finish(n_view(block), f_sems, step, spreads[step])
         total = jnp.zeros((2 * piece, rows), jnp.float32)
         tokens = n_all[block].reshape(rows, model)
@@ -448,9 +490,20 @@
     return pl.pallas_call(
         functools.partial(layer_kernel, grp_count, sp_count, tp_count),
         out_shape=jax.ShapeDtypeStruct((rows, model), half),
-        in_specs=[pl.BlockSpec(memory_space=pltpu.VMEM)] * 10,
+        in_specs=[pl.BlockSpec(memory_space=pl.ANY)] * 10,
         out_specs=pl.BlockSpec(memory_space=pltpu.VMEM),
         scratch_shapes=[
+            pltpu.VMEM((rows, columns), half),
+            pltpu.VMEM((rows, columns), half),
+            pltpu.VMEM((rows, columns), half),
+            pltpu.VMEM((head_count, rows), half),
+            pltpu.VMEM((quarter, model), half),
+            pltpu.VMEM((columns, model), half),
+            pltpu.VMEM((model,), half),
+            pltpu.VMEM((slab, hidden), half),
+            pltpu.VMEM((slab, hidden), half),
+            pltpu.VMEM((hidden, slab), half),
+            dma((10,)),
             pltpu.VMEM((n, rows, columns), half),
             pltpu.VMEM((n, rows, columns), half),
             pltpu.VMEM((n, head_count, rows), half),
@@ -479,7 +532,7 @@
             dma((2, 3, 1)),
         ],
         compiler_params=pltpu.CompilerParams(
-            collective_id=0, has_side_effects=True, vmem_limit_bytes=48 * 1024 * 1024
+            collective_id=0, has_side_effects=True, vmem_limit_bytes=67_043_328
         ),
     )(
         queries,
@@ -488,7 +541,7 @@
         key_bias,
         residual,
         out_weight,
-        norm_gain.reshape(1, model),
+        norm_gain,
         gate_weight,
         up_weight,
         down_weight,

time: 89.3 us -> 82 us (0.918); the launches traced: 87.7 us -> 81.8 us
  local copies, waits for them, and re-layouts: 9.25 us -> 1.88 us
  Pallas kernels: 78.4 us -> 79.9 us
    unnamed x19 -> x1, local copies, waits for them, and re-layouts: 8.55 us -> 1.88 us
    pallas_call x1, Pallas kernels: 78.4 us -> 79.9 us  [fused_body(): pl.pallas_call(functools.partial(layer_kernel, grp_count, sp_count, tp_co...]
where the time goes in v2:
time: 82 us; the launch traced here: 81.8 us
  Pallas kernels  79.9 us (97%)
  local copies, waits for them, and re-layouts  1.88 us (2%)
    pallas_call x1, Pallas kernels, fused_body(): pl.pallas_call(functools.partial(layer_kernel, grp_count, sp_count, tp_co...  79.9 us
    unnamed x1, local copies, waits for them, and re-layouts  1.88 us

profile of v2, /device:TPU:0, one launch (start us, length us, event | category | flops | bytes accessed | tf_op | source)
XLA Modules:
  0.0 81.8 jit_solution(9314194471629435508)
XLA Ops:
  0.0 79.9 %shard_map.100 = bf16[128,2048]{1,0:T(8,128)(2,1)} custom-call(bf16[128,128]{1,0:T(8,128)(2,1)} %q_in.1, bf16[128,128]{1,0:T(8,128)(2,1)} %k_in.1, bf16[128,128]{1,0:T(8,128)(2,1)} %v_in.1, bf16[2,128]{1,0:T(2,128)(2,1)} %bias_in.1, bf16[128,2048]{1,0:T(8,128)(2,1)} %res_in.1, bf16[128,2048]{1,0:T(8,128)(2,1)} %ow_in.1, bf16[2048]{0:T(1024)(128)(2,1)} %gain_in.1, ...), custom_call_target="tpu_custom_call" | custom-call | tf_op jit(solution)/shard_map/pallas_call | solution.py:490
  79.9 1.9 %copy.12 = bf16[128,2048]{1,0:T(8,128)(2,1)} copy(bf16[128,2048]{1,0:T(8,128)(2,1)} %shard_map.100) | data formatting | bytes 1048576

commit v3 on v2

--- a/solution.py
+++ b/solution.py
@@ -196,7 +196,7 @@
     piece = gate_ref.shape[1] // sp_count
     head_count = bias_ref.shape[0]
     width = q_ref.shape[1] // head_count
-    sends = []
+    sends, guarded = [], []
 
     def sp_peer(step):
         return lax.rem(s + step + sp_count, sp_count)
@@ -353,70 +353,138 @@
         wide * lax.rsqrt(mean_square + norm_eps) * gain_ref[...].astype(jnp.float32).reshape(1, model)
     ).astype(jnp.bfloat16)
 
-    n_copies = {}
-    for step in range(1, sp_count):
-        n_copies[step] = launch(
-            n_all.at[s, t], n_all.at[s, t], n_sems, (step - 1,), (g, sp_peer(step), t)
+    up, down = 0, 1
+    slots = [(step, way) for step in range(1, sp_count) for way in (up, down)]
+
+    def place_of(origin, step, way):
+        return origin - step if way == up else origin + step
+
+    def inside(place):
+        return (place >= 0) & (place < sp_count)
+
+    def wrap(place):
+        return lax.rem(place + 2 * sp_count, sp_count)
+
+    def chain_copy(view, sems, way, hop, index):
+        onward = wrap(s + 1 if way == up else s - 1)
+        return copy(view, view, sems, (way, hop) + index, (g, onward, t))
+
+    def chain_start(view, sems, way, hop, index, valid):
+        going = valid & inside(s + 1 if way == up else s - 1)
+        made = chain_copy(view, sems, way, hop, index)
+        pl.when(going)(made.start)
+        guarded.append((going, made))
+
+    def spread(ref, sems, index, valid):
+        first = (
+            copy(ref(t), ref(t), sems, (0, index), (g, s, far_mate)),
+            copy(ref(t), ref(t), sems, (1, index), (g, s, core_mate)),
         )
-
-    def spread(ref, sems, index):
-        return (
-            launch(ref(t), ref(t), sems, (0, index), (g, s, far_mate)),
-            launch(ref(t), ref(t), sems, (1, index), (g, s, core_mate)),
-        )
-
-    def finish(ref, sems, index, first):
-        first[0].wait_recv()
-        relayed = launch(ref(far_mate), ref(far_mate), sems, (2, index), (g, s, core_mate))
-        first[1].wait_recv()
-        relayed.wait_recv()
+        for made in first:
+            pl.when(valid)(made.start)
+            guarded.append((valid, made))
+        return first
+
+    def finish(ref, sems, index, first, valid):
+        relayed = copy(ref(far_mate), ref(far_mate), sems, (2, index), (g, s, core_mate))
+
+        @pl.when(valid)
+        def _():
+            first[0].wait_recv()
+            relayed.start()
+            first[1].wait_recv()
+            relayed.wait_recv()
+
+        guarded.append((valid, relayed))
 
     def n_view(block):
         return lambda place: n_all.at[block, place]
 
-    spreads = {0: spread(n_view(s), f_sems, 0)}
+    def slot_number(slot):
+        return 0 if slot is None else 1 + slots.index(slot)
+
+    always = s >= 0
+    spreads = {}
+
+    def arrive(slot):
+        step, way = slot
+        origin = place_of(s, step, way)
+        valid, block = inside(origin), wrap(origin)
+        view = n_all.at[block, t]
+        pl.when(valid)(chain_copy(view, n_sems, way, step - 1, ()).wait_recv)
+        if step < sp_count - 1:
+            chain_start(view, n_sems, way, step, (), valid)
+        spreads[slot] = spread(n_view(block), f_sems, slot_number(slot), valid)
+
+    def process(slot):
+        origin = s if slot is None else place_of(s, *slot)
+        valid = always if slot is None else inside(origin)
+        block = wrap(origin)
+        number = slot_number(slot)
+        finish(n_view(block), f_sems, number, spreads[slot], valid)
+
+        @pl.when(valid)
+        def _():
+            total = jnp.zeros((2 * piece, rows), jnp.float32)
+            tokens = n_all[block].reshape(rows, model)
+            for part in range(sp_count):
+                total = total + contract(
+                    w_all[part].reshape(2 * piece, slab),
+                    tokens[:, part * slab : (part + 1) * slab],
+                    (1, 1),
+                )
+            gate_pre, up_pre = total[:piece], total[piece:]
+            h_all[block, s] = (gate_pre / (1.0 + jnp.exp(-gate_pre)) * up_pre).astype(jnp.bfloat16)
+
+        for way in (up, down):
+            chain_start(h_all.at[block, s], h_sems, way, 0, (number,), valid)
+
+    def hop_on(slot, step, way):
+        if slot is not None and slot[1] == way and slot[0] + step >= sp_count:
+            return
+        source = place_of(s, step, way)
+        target = source if slot is None else place_of(source, *slot)
+        valid = inside(source) & inside(target)
+        view, index = h_all.at[wrap(target), wrap(source)], (slot_number(slot),)
+        pl.when(valid)(chain_copy(view, h_sems, way, step - 1, index).wait_recv)
+        if step < sp_count - 1:
+            chain_start(view, h_sems, way, step, index, valid)
+
+    def hop_all(stage):
+        for distance in range(stage):
+            step = stage - distance
+            if step < sp_count and distance < sp_count:
+                for slot in [None] if distance == 0 else [(distance, up), (distance, down)]:
+                    for way in (up, down):
+                        hop_on(slot, step, way)
+
+    for way in (up, down):
+        chain_start(n_all.at[s, t], n_sems, way, 0, (), always)
+    spreads[None] = spread(n_view(s), f_sems, 0, always)
     y_copies = []
     for step in range(1, sp_count):
         w_copies[step].wait_recv()
         view = w_all.at[sp_peer(-step), g]
         y_copies.append(launch(view, view, wy_sems, (step - 1,), (1 - g, s, t)))
-
-    def pass_on(step):
-        if step < sp_count:
-            n_copies[step].wait_recv()
-            spreads[step] = spread(n_view(sp_peer(-step)), f_sems, step)
-
-    pass_on(1)
+    arrive((1, up))
+    arrive((1, down))
     for made in y_copies:
         made.wait_recv()
-
-    h_copies = {}
-    for step in range(sp_count):
-        block = sp_peer(-step)
-        if step:
-            pass_on(step + 1)
-        finish(n_view(block), f_sems, step, spreads[step])
-        total = jnp.zeros((2 * piece, rows), jnp.float32)
-        tokens = n_all[block].reshape(rows, model)
-        for part in range(sp_count):
-            total = total + contract(
-                w_all[part].reshape(2 * piece, slab),
-                tokens[:, part * slab : (part + 1) * slab],
-                (1, 1),
-            )
-        gate_pre, up_pre = total[:piece], total[piece:]
-        h_all[block, s] = (gate_pre / (1.0 + jnp.exp(-gate_pre)) * up_pre).astype(jnp.bfloat16)
-        for hop in range(1, sp_count):
-            h_copies[step, hop] = launch(
-                h_all.at[block, s], h_all.at[block, s], h_sems, (step, hop - 1), (g, sp_peer(hop), t)
-            )
+    process(None)
+    for stage in range(1, sp_count):
+        for way in (up, down):
+            if stage < sp_count - 1:
+                arrive((stage + 1, way))
+        for way in (up, down):
+            process((stage, way))
+        hop_all(stage)
+    for stage in range(sp_count, 2 * sp_count - 1):
+        hop_all(stage)
 
     d_copies = {}
     order = list(range(1, sp_count)) + [0]
     for step in order:
         block = sp_peer(-step)
-        for hop in range(1, sp_count):
-            h_copies[(step - hop) % sp_count, hop].wait_recv()
         hidden = h_all[block].reshape(sp_count * piece, rows)
         dbuf[block] = contract(hidden, down_ref[...], (0, 0)).astype(jnp.bfloat16)
         for hop in range(1, tp_count):
@@ -453,9 +521,11 @@
     def out_view(place):
         return out_ref.at[own_rows(place)]
 
-    finish(out_view, o_sems, 0, spread(out_view, o_sems, 0))
+    finish(out_view, o_sems, 0, spread(out_view, o_sems, 0, always), always)
     for made in sends:
         made.wait_send()
+    for valid, made in guarded:
+        pl.when(valid)(made.wait_send)
     for step in range(1, sp_count):
 
         @pl.when(s + step < sp_count)
@@ -524,9 +594,9 @@
             dma((2, n)),
             dma((2, n)),
             dma((2, m)),
-            dma((2, n)),
-            dma((2, 3, sp_count)),
-            dma((2, sp_count, n)),
+            dma((2, 2, n)),
+            dma((2, 3, 2 * n + 1)),
+            dma((2, 2, n, 2 * n + 1)),
             dma((2, sp_count, m)),
             dma((2, n)),
             dma((2, 3, 1)),

time: 82 us -> 77.8 us (0.949)
  Pallas kernels: 79.9 us -> 75.7 us
    pallas_call x1, Pallas kernels: 79.9 us -> 75.7 us  [fused_body(): pl.pallas_call(functools.partial(layer_kernel, grp_count, sp_count, tp_co...]
where the time goes in v3:
time: 77.8 us; the launch traced here: 77.6 us
  Pallas kernels  75.7 us (97%)
  local copies, waits for them, and re-layouts  1.88 us (2%)
    pallas_call x1, Pallas kernels, fused_body(): pl.pallas_call(functools.partial(layer_kernel, grp_count, sp_count, tp_co...  75.7 us
    unnamed x1, local copies, waits for them, and re-layouts  1.88 us

profile of v3, /device:TPU:0, one launch (start us, length us, event | category | flops | bytes accessed | tf_op | source)
XLA Modules:
  0.0 77.6 jit_solution(13700037731617743958)
XLA Ops:
  0.0 75.7 %shard_map.100 = bf16[128,2048]{1,0:T(8,128)(2,1)} custom-call(bf16[128,128]{1,0:T(8,128)(2,1)} %q_in.1, bf16[128,128]{1,0:T(8,128)(2,1)} %k_in.1, bf16[128,128]{1,0:T(8,128)(2,1)} %v_in.1, bf16[2,128]{1,0:T(2,128)(2,1)} %bias_in.1, bf16[128,2048]{1,0:T(8,128)(2,1)} %res_in.1, bf16[128,2048]{1,0:T(8,128)(2,1)} %ow_in.1, bf16[2048]{0:T(1024)(128)(2,1)} %gain_in.1, ...), custom_call_target="tpu_custom_call" | custom-call | tf_op jit(solution)/shard_map/pallas_call | solution.py:560
  75.7 1.9 %copy.12 = bf16[128,2048]{1,0:T(8,128)(2,1)} copy(bf16[128,2048]{1,0:T(8,128)(2,1)} %shard_map.100) | data formatting | bytes 1048576

commit v4 on v3

--- a/solution.py
+++ b/solution.py
@@ -176,6 +176,7 @@
     h_all,
     dbuf,
     rdown,
+    psend,
     zsend,
     zin,
     kv_sems,
@@ -487,22 +488,28 @@
         block = sp_peer(-step)
         hidden = h_all[block].reshape(sp_count * piece, rows)
         dbuf[block] = contract(hidden, down_ref[...], (0, 0)).astype(jnp.bfloat16)
-        for hop in range(1, tp_count):
-            dest = tp_peer(hop)
+        for hop, share in enumerate((lax.rem(core_mate + 2, 4), core_mate)):
             d_copies[step, hop] = launch(
-                dbuf.at[block, own_rows(dest)],
-                rdown.at[hop - 1, step],
+                dbuf.at[block, own_rows(share)],
+                rdown.at[hop, step],
                 d_sems,
-                (step, hop - 1),
-                (g, s, dest),
+                (step, hop),
+                (g, s, core_mate),
             )
+    for step in order:
+        d_copies[step, 0].wait_recv()
+        pair = dbuf[sp_peer(-step), own_rows(far_mate), :].astype(jnp.float32)
+        psend[step] = (pair + rdown[0, step].astype(jnp.float32)).astype(jnp.bfloat16)
+        d_copies[step, 2] = launch(
+            psend.at[step], rdown.at[2, step], d_sems, (step, 2), (g, s, far_mate)
+        )
     z_copies = {}
     for step in order:
         block = sp_peer(-step)
         summed = dbuf[block, own_rows(t), :].astype(jnp.float32)
-        for hop in range(1, tp_count):
+        for hop in (1, 2):
             d_copies[step, hop].wait_recv()
-            summed = summed + rdown[hop - 1, step].astype(jnp.float32)
+            summed = summed + rdown[hop, step].astype(jnp.float32)
         if step:
             zsend[step - 1] = summed.astype(jnp.bfloat16)
             z_copies[step] = launch(
@@ -588,6 +595,7 @@
             pltpu.VMEM((sp_count, sp_count, piece, rows), half),
             pltpu.VMEM((sp_count, rows, slab), half),
             pltpu.VMEM((m, sp_count, quarter, slab), half),
+            pltpu.VMEM((sp_count, quarter, slab), half),
             pltpu.VMEM((n, quarter, slab), half),
             pltpu.VMEM((sp_count, quarter, slab), half),
             dma((2, 3, n)),

time: 77.8 us -> 78.3 us (level)
  no operation moved by 1% of the time
where the time goes in v4:
time: 78.3 us; the launch traced here: 78.1 us
  Pallas kernels  76.2 us (97%)
  local copies, waits for them, and re-layouts  1.88 us (2%)
    pallas_call x1, Pallas kernels, fused_body(): pl.pallas_call(functools.partial(layer_kernel, grp_count, sp_count, tp_co...  76.2 us
    unnamed x1, local copies, waits for them, and re-layouts  1.88 us

profile of v4, /device:TPU:0, one launch (start us, length us, event | category | flops | bytes accessed | tf_op | source)
XLA Modules:
  0.0 78.1 jit_solution(13066046688622296240)
XLA Ops:
  0.0 76.2 %shard_map.100 = bf16[128,2048]{1,0:T(8,128)(2,1)} custom-call(bf16[128,128]{1,0:T(8,128)(2,1)} %q_in.1, bf16[128,128]{1,0:T(8,128)(2,1)} %k_in.1, bf16[128,128]{1,0:T(8,128)(2,1)} %v_in.1, bf16[2,128]{1,0:T(2,128)(2,1)} %bias_in.1, bf16[128,2048]{1,0:T(8,128)(2,1)} %res_in.1, bf16[128,2048]{1,0:T(8,128)(2,1)} %ow_in.1, bf16[2048]{0:T(1024)(128)(2,1)} %gain_in.1, ...), custom_call_target="tpu_custom_call" | custom-call | tf_op jit(solution)/shard_map/pallas_call | solution.py:567
  76.2 1.9 %copy.12 = bf16[128,2048]{1,0:T(8,128)(2,1)} copy(bf16[128,2048]{1,0:T(8,128)(2,1)} %shard_map.100) | data formatting | bytes 1048576
